TPU v7x, 32 devices: a whole 2x2x4 slice. The times are simulated.
32 devices in a mesh: grp: 2 (over y), fs: 4 (over z), tp: 4 (over x, core).
Axes of the slice: x: 2, y: 2, z: 4, core: 2. Of those that a mesh axis runs over, the one named last changes fastest.
Arguments:
- tokens: bfloat16 [8192, 2048], P(('grp', 'fs', 'tp')), parts along dimension 0, may hold values from -6 to 6
- first_gain: float32 [2048], replicated, may hold values from 0.1 to 1.9
- mixer_gain: float32 [2048], replicated, may hold values from 0.1 to 1.9
- gate_weight: bfloat16 [2048, 4608], P('fs', 'tp'), may hold values from -0.125 to 0.125
- up_weight: bfloat16 [2048, 4608], P('fs', 'tp'), may hold values from -0.125 to 0.125
- down_weight: bfloat16 [4608, 2048], P('tp', 'fs'), may hold values from -0.09375 to 0.09375
- query_weight: bfloat16 [2048, 2048], P('fs', 'tp'), may hold values from -0.125 to 0.125
- key_weight: bfloat16 [2048, 2048], P('fs', 'tp'), may hold values from -0.125 to 0.125
- value_weight: bfloat16 [2048, 4096], P('fs', 'tp'), may hold values from -0.125 to 0.125
- head_gain: float32 [4096], P('tp'), may hold values from 0.1 to 1.9
- out_weight: bfloat16 [4096, 2048], P('tp', 'fs'), may hold values from -0.09375 to 0.09375
- log_decay: float32 [2, 8], P(None, 'tp'), may hold values from -0.03125 to 0, as said below
Outputs:
- updated: bfloat16 [8192, 2048], P(('grp', 'fs', 'tp')), parts along dimension 0
There are 2 independent parts, one for each index of `grp`. A program takes and returns all parts, laid end to end along the dimension named above; an argument that names none is the same for every part. Nothing has to cross between parts.
Inputs may be any that keep to these rules, and one draw needn't show every extreme that they name: `log_decay`: log decay per step of each direction (forward, then backward) and head.
All inputs are finite; a program needn't handle non-finite values.
Results may differ from a plain program's by a relative error of at most 0.02.
Values may be sent and summed in bfloat16 or wider, within the bound.
A program may use at most 64 MiB of HBM per device.

v0:
```python
import functools

import jax
import jax.numpy as jnp
from jax import lax
from jax.experimental import pallas as pl
from jax.experimental.pallas import tpu as pltpu
from jax.sharding import PartitionSpec as P

DK = 256
DV = 512
EPS = 1e-06
LANES = 128


def norm_rows(values, gain):
    widened = values.astype(jnp.float32)
    factor = lax.rsqrt(jnp.mean(widened * widened, axis=-1, keepdims=True) + EPS)
    return (widened * factor * gain).astype(jnp.bfloat16)


def tile_of(width, top):
    best = width
    for tile in range(LANES, top + 1, LANES):
        if width % tile == 0:
            best = tile
    return best


def cost(flops, *arrays):
    return pl.CostEstimate(
        flops=flops,
        transcendentals=0,
        bytes_accessed=sum(a.size * a.dtype.itemsize for a in arrays),
    )


def retain_kernel(decay_ref, query_ref, key_ref, value_ref, gain_ref, out_ref):
    head, block = pl.program_id(0), pl.program_id(1)
    tall, length = query_ref.shape[0], key_ref.shape[0]
    scores = lax.dot_general(
        query_ref[...], key_ref[...], (((1,), (1,)), ((), ())),
        preferred_element_type=jnp.float32,
    )
    here = lax.broadcasted_iota(jnp.int32, (tall, length), 0) + block * tall
    there = lax.broadcasted_iota(jnp.int32, (tall, length), 1)
    distance = (here - there).astype(jnp.float32)
    rate = jnp.where(distance >= 0, decay_ref[0, head], -decay_ref[1, head])
    decay = jnp.exp(rate * distance) * jnp.where(
        distance == 0, 2.0 * DK ** (-0.5), DK ** (-0.5)
    )
    outputs = jnp.dot(
        (scores * decay).astype(jnp.bfloat16), value_ref[...],
        preferred_element_type=jnp.float32,
    )
    centered = outputs - jnp.mean(outputs, axis=-1, keepdims=True)
    variance = jnp.mean(centered * centered, axis=-1, keepdims=True)
    out_ref[...] = (centered * lax.rsqrt(variance + EPS) * gain_ref[...]).astype(jnp.bfloat16)


def retain(queries, key_rows, value_rows, head_gain, log_decay):
    length, width = value_rows.shape
    tall = tile_of(length, 256)
    return pl.pallas_call(
        retain_kernel,
        grid=(width // DV, length // tall),
        in_specs=[
            pl.BlockSpec(memory_space=pltpu.SMEM),
            pl.BlockSpec((tall, DK), lambda h, i: (i, h)),
            pl.BlockSpec((length, DK), lambda h, i: (0, h)),
            pl.BlockSpec((length, DV), lambda h, i: (0, h)),
            pl.BlockSpec((1, DV), lambda h, i: (0, h)),
        ],
        out_specs=pl.BlockSpec((tall, DV), lambda h, i: (i, h)),
        out_shape=jax.ShapeDtypeStruct((length, width), jnp.bfloat16),
        cost_estimate=cost(3 * 2 * length * length * width // 2, queries, value_rows),
    )(log_decay, queries, key_rows, value_rows, head_gain.reshape(1, -1))


def dot(left, right):
    return jnp.dot(left, right, preferred_element_type=jnp.float32)


def layer_kernel(size, *refs):
    (tokens, first_gain, mixer_gain, head_gain, decay) = refs[:5]
    sources, updated = refs[5:12], refs[12]
    weights = refs[13:20]
    (rows_one, rows_two, hidden, part, queries, key_rows, value_rows, flat, after_first,
     far_one, near_one, cross_one, pair_one, far_two, near_two, cross_two, pair_two,
     local_sem, z_recv, z_send, z_left, y_recv, y_send, tp_send, tp_recv) = refs[20:]
    gate, up, down, query_w, key_w, value_w, out_w = weights
    column_split = (False, False, True, False, False, False, True)
    group, z, spot = lax.axis_index("grp"), lax.axis_index("fs"), lax.axis_index("tp")
    chip, core = spot // 2, spot % 2
    mate = chip * 2 + (1 - core)
    peer = (1 - chip) * 2 + core
    last = size - 1
    band = tokens.shape[0]

    def shard_at(w, shard, side=None):
        tall, wide = sources[w].shape
        height = tall if side is None else tall // 2
        start = 0 if side is None else side * height
        if column_split[w]:
            return weights[w].at[
                pl.ds(pl.multiple_of(start, height), height),
                pl.ds(pl.multiple_of(shard * wide, wide), wide),
            ]
        return weights[w].at[pl.ds(pl.multiple_of(shard * tall + start, height), height), :]

    def own_copy(w):
        return pltpu.make_async_copy(sources[w], shard_at(w, z), local_sem.at[w])

    def along(w, shard, to, send_sem):
        block = shard_at(w, shard, group)
        return pltpu.make_async_remote_copy(
            src_ref=block, dst_ref=block, send_sem=send_sem, recv_sem=z_recv.at[w, shard],
            device_id={"fs": to}, device_id_type=pl.DeviceIdType.MESH,
        )

    def across(w, shard, side):
        block = shard_at(w, shard, side)
        return pltpu.make_async_remote_copy(
            src_ref=block, dst_ref=block, send_sem=y_send.at[w, shard],
            recv_sem=y_recv.at[w, shard],
            device_id={"grp": 1 - group}, device_id_type=pl.DeviceIdType.MESH,
        )

    def send_tp(source, target, number, to):
        return pltpu.make_async_remote_copy(
            src_ref=source, dst_ref=target, send_sem=tp_send.at[number],
            recv_sem=tp_recv.at[number],
            device_id={"tp": to}, device_id_type=pl.DeviceIdType.MESH,
        )

    def start(w):
        own_copy(w).wait()

        @pl.when(z < last)
        def _():
            along(w, z, z + 1, z_send.at[w, z]).start()

        @pl.when(z > 0)
        def _():
            along(w, z, z - 1, z_left.at[w]).start()

    def step(w, k):
        @pl.when(z - k >= 0)
        def _():
            copy = along(w, z - k, z + 1, z_send.at[w, z - k])
            copy.wait_recv()

            @pl.when(z < last)
            def _():
                copy.start()

            across(w, z - k, group).start()

        @pl.when(z + k <= last)
        def _():
            copy = along(w, z + k, z - 1, z_send.at[w, z + k])
            copy.wait_recv()

            @pl.when(z > 0)
            def _():
                copy.start()

            across(w, z + k, group).start()

    def steps(w):
        for k in range(1, size):
            step(w, k)

    def finish(w):
        for k in range(1, size):
            @pl.when(z - k >= 0)
            def _():
                across(w, z - k, 1 - group).wait_recv()

            @pl.when(z + k <= last)
            def _():
                across(w, z + k, 1 - group).wait_recv()

    def drain(w):
        @pl.when(z < last)
        def _():
            along(w, z, z + 1, z_send.at[w, z]).wait_send()

        @pl.when(z > 0)
        def _():
            along(w, z, z - 1, z_left.at[w]).wait_send()

        for k in range(1, size):
            @pl.when(z - k >= 0)
            def _():
                @pl.when(z < last)
                def _():
                    along(w, z - k, z + 1, z_send.at[w, z - k]).wait_send()

                across(w, z - k, group).wait_send()

            @pl.when(z + k <= last)
            def _():
                @pl.when(z > 0)
                def _():
                    along(w, z + k, z - 1, z_send.at[w, z + k]).wait_send()

                across(w, z + k, group).wait_send()

    def band_of(ref, place):
        return ref.at[pl.ds(pl.multiple_of(place * band, band), band), :]

    def by_chunks(body):
        tall = band // 4

        def chunk(i, carry):
            body(pl.multiple_of(i * tall, tall), tall)
            return carry

        lax.fori_loop(0, 4, chunk, 0)

    def normed_into(rows, source, gain):
        def body(first, tall):
            start_row = pl.multiple_of(spot * band + first, tall)
            rows[pl.ds(start_row, tall), :] = norm_rows(source[pl.ds(first, tall), :], gain[...])

        by_chunks(body)

    def gather_start(rows, base):
        mine = band_of(rows, spot)
        send_tp(mine, mine, base + 1, peer).start()
        send_tp(mine, mine, base, mate).start()

    def gather_forward(rows, base):
        theirs = band_of(rows, peer)
        send_tp(theirs, theirs, base + 1, peer).wait_recv()
        send_tp(theirs, theirs, base + 2, mate).start()

    def gather_end(rows, base):
        near, beyond = band_of(rows, mate), band_of(rows, (1 - chip) * 2 + (1 - core))
        send_tp(near, near, base, mate).wait_recv()
        send_tp(beyond, beyond, base + 2, mate).wait_recv()

    def gather_drain(rows, base):
        for number, to in ((0, mate), (1, peer), (2, mate)):
            send_tp(band_of(rows, spot), band_of(rows, spot), base + number, to).wait_send()

    def product(target, source, weight, first, tall, wide):
        def tile(t, carry):
            columns = pl.ds(pl.multiple_of(t * wide, wide), wide)
            target[pl.ds(first, tall), columns] = dot(
                source[pl.ds(first, tall), :], weight[:, columns]
            ).astype(jnp.bfloat16)
            return carry

        lax.fori_loop(0, weight.shape[1] // wide, tile, 0)

    def scatter_far(far, base):
        send_tp(band_of(part, (1 - chip) * 2 + (1 - core)), far, base, mate).start()

    def scatter_near(near, base):
        send_tp(band_of(part, mate), near, base + 1, mate).start()

    def scatter_cross(far, pair, cross, base):
        send_tp(far, far, base, mate).wait_recv()

        def body(first, tall):
            from_row = pl.multiple_of(peer * band + first, tall)
            pair[pl.ds(first, tall), :] = (
                part[pl.ds(from_row, tall), :].astype(jnp.float32)
                + far[pl.ds(first, tall), :].astype(jnp.float32)
            ).astype(jnp.bfloat16)

        by_chunks(body)
        send_tp(pair, cross, base + 2, peer).start()

    def scatter_end(residual, near, cross, scale, target, base):
        send_tp(near, near, base + 1, mate).wait_recv()
        send_tp(cross, cross, base + 2, peer).wait_recv()

        def body(first, tall):
            here = pl.ds(first, tall)
            own_row = pl.multiple_of(spot * band + first, tall)
            total = part[pl.ds(own_row, tall), :].astype(jnp.float32)
            total = total + near[here, :].astype(jnp.float32)
            total = total + cross[here, :].astype(jnp.float32)
            target[here, :] = (
                residual[here, :].astype(jnp.float32) + scale * total
            ).astype(jnp.bfloat16)

        by_chunks(body)

    def scatter_drain(near, base):
        for number, to in ((0, mate), (1, mate), (2, peer)):
            send_tp(near, near, base + number, to).wait_send()

    half_rows = 2 * band
    far_rows = pl.multiple_of((1 - chip) * half_rows, half_rows)
    chip_rows = pl.multiple_of(chip * half_rows, half_rows)

    def gated_rows(first):
        wide = tile_of(gate.shape[1], 384)

        def tile(t, carry):
            columns = pl.ds(pl.multiple_of(t * wide, LANES), wide)
            rows = rows_one[pl.ds(first, half_rows), :]
            gate_sum = dot(rows, gate[:, columns])
            up_sum = dot(rows, up[:, columns])
            hidden[pl.ds(first, half_rows), columns] = (
                gate_sum / (1.0 + jnp.exp(-gate_sum)) * up_sum
            ).astype(jnp.bfloat16)
            return carry

        lax.fori_loop(0, gate.shape[1] // wide, tile, 0)

    def retain_head(head):
        length = key_rows.shape[0]
        tall = tile_of(length, 256)
        keyed = slice(head * DK, (head + 1) * DK)
        valued = slice(head * DV, (head + 1) * DV)

        def tile(i, carry):
            first = pl.multiple_of(i * tall, tall)
            scores = lax.dot_general(
                queries[pl.ds(first, tall), keyed], key_rows[:, keyed],
                (((1,), (1,)), ((), ())), preferred_element_type=jnp.float32,
            )
            here = lax.broadcasted_iota(jnp.int32, (tall, length), 0) + first
            there = lax.broadcasted_iota(jnp.int32, (tall, length), 1)
            distance = (here - there).astype(jnp.float32)
            rate = jnp.where(distance >= 0, decay[0, head], -decay[1, head])
            factor = jnp.where(distance == 0, 2.0 * DK ** (-0.5), DK ** (-0.5))
            weighted = (scores * (jnp.exp(rate * distance) * factor)).astype(jnp.bfloat16)
            outputs = dot(weighted, value_rows[:, valued])
            centered = outputs - jnp.mean(outputs, axis=-1, keepdims=True)
            variance = jnp.mean(centered * centered, axis=-1, keepdims=True)
            flat[pl.ds(first, tall), valued] = (
                centered * lax.rsqrt(variance + EPS) * head_gain[:, valued]
            ).astype(jnp.bfloat16)
            return carry

        lax.fori_loop(0, length // tall, tile, 0)

    for w in range(7):
        own_copy(w).start()
    barrier = pltpu.get_barrier_semaphore()

    def greet(**where):
        pl.semaphore_signal(
            barrier, inc=1, device_id=where, device_id_type=pl.DeviceIdType.MESH
        )

    greet(tp=mate)
    greet(tp=peer)
    greet(grp=1 - group)

    @pl.when(z > 0)
    def _():
        greet(fs=z - 1)

    @pl.when(z < last)
    def _():
        greet(fs=z + 1)

    pl.semaphore_wait(barrier, 3 + jnp.minimum(z, 1) + jnp.minimum(last - z, 1))

    start(0)
    start(1)
    normed_into(rows_one, tokens, first_gain)
    gather_start(rows_one, 0)
    step(0, 1)
    start(2)
    for k in range(2, size):
        step(0, k)
    gather_forward(rows_one, 0)
    step(1, 1)
    start(3)
    for k in range(2, size):
        step(1, k)
    gather_end(rows_one, 0)
    finish(0)
    step(2, 1)
    start(4)
    finish(1)
    gated_rows(0)
    step(2, 2)
    gated_rows(half_rows)
    for k in range(3, size):
        step(2, k)
    step(3, 1)
    start(5)
    finish(2)
    product(part, hidden, down, far_rows, half_rows, 512)
    scatter_far(far_one, 3)
    product(part, hidden, down, chip_rows, half_rows, 512)
    scatter_near(near_one, 3)
    scatter_cross(far_one, pair_one, cross_one, 3)
    for k in range(2, size):
        step(3, k)
    scatter_end(tokens, near_one, cross_one, 0.5, after_first, 3)
    normed_into(rows_two, after_first, mixer_gain)
    gather_start(rows_two, 6)
    step(4, 1)
    start(6)
    for k in range(2, size):
        step(4, k)
    step(5, 1)
    gather_forward(rows_two, 6)
    step(5, 2)
    gather_end(rows_two, 6)
    finish(3)
    for first in (0, half_rows):
        product(queries, rows_two, query_w, first, half_rows, 512)
    for k in range(3, size):
        step(5, k)
    step(6, 1)
    finish(4)
    for first in (0, half_rows):
        product(key_rows, rows_two, key_w, first, half_rows, 512)
    finish(5)
    product(value_rows, rows_two, value_w, 0, half_rows, 512)
    step(6, 2)
    product(value_rows, rows_two, value_w, half_rows, half_rows, 512)
    for k in range(3, size):
        step(6, k)
    for head in range(value_rows.shape[1] // DV):
        retain_head(head)
    finish(6)
    scatter_drain(near_one, 3)
    product(part, flat, out_w, far_rows, half_rows, 512)
    scatter_far(far_two, 9)
    product(part, flat, out_w, chip_rows, half_rows, 512)
    scatter_near(near_two, 9)
    scatter_cross(far_two, pair_two, cross_two, 9)
    scatter_end(after_first, near_two, cross_two, 1.0, updated, 9)
    for w in range(7):
        drain(w)
    gather_drain(rows_one, 0)
    gather_drain(rows_two, 6)
    scatter_drain(near_two, 9)


def shards_fused(
    size, tokens, first_gain, mixer_gain, gate_weight, up_weight, down_weight,
    query_weight, key_weight, value_weight, head_gain, out_weight, log_decay,
):
    band, depth = tokens.shape
    length = 4 * band
    sources = (
        gate_weight, up_weight, down_weight, query_weight, key_weight, value_weight, out_weight
    )

    def held(*shape):
        return pltpu.VMEM(shape, jnp.bfloat16)

    whole = [
        held(w.shape[0], w.shape[1] * size) if place in (2, 6) else held(w.shape[0] * size, w.shape[1])
        for place, w in enumerate(sources)
    ]
    dma = pltpu.SemaphoreType.DMA
    count = len(sources)
    in_vmem = pl.BlockSpec(memory_space=pltpu.VMEM)
    return pl.pallas_call(
        functools.partial(layer_kernel, size),
        in_specs=[in_vmem] * 4
        + [pl.BlockSpec(memory_space=pltpu.SMEM)]
        + [pl.BlockSpec(memory_space=pl.ANY)] * count,
        out_specs=in_vmem,
        out_shape=jax.ShapeDtypeStruct(tokens.shape, tokens.dtype),
        scratch_shapes=whole
        + [
            held(length, depth), held(length, depth), held(length, gate_weight.shape[1]),
            held(length, depth), held(length, query_weight.shape[1]),
            held(length, key_weight.shape[1]), held(length, value_weight.shape[1]),
            held(length, value_weight.shape[1]), held(band, depth),
        ]
        + [held(band, depth)] * 8
        + [
            dma((count,)), dma((count, size)), dma((count, size)), dma((count,)),
            dma((count, size)), dma((count, size)), dma((12,)), dma((12,)),
        ],
        compiler_params=pltpu.CompilerParams(
            collective_id=0, has_side_effects=True, vmem_limit_bytes=67_000_000
        ),
    )(
        tokens, first_gain.reshape(1, -1), mixer_gain.reshape(1, -1), head_gain.reshape(1, -1),
        log_decay, *sources,
    )


def shards_gathered(
    tokens, first_gain, mixer_gain, gate_weight, up_weight, down_weight,
    query_weight, key_weight, value_weight, head_gain, out_weight, log_decay,
):
    def rows_of(weight):
        return lax.all_gather(weight, "fs", axis=0, tiled=True)

    def columns_of(weight):
        return lax.all_gather(weight, "fs", axis=1, tiled=True)

    def times(left, right):
        return jnp.dot(left, right, preferred_element_type=jnp.float32)

    normed = norm_rows(tokens, first_gain)
    gathered = lax.all_gather(normed, "tp", axis=0, tiled=True)
    gate_sum = times(gathered, rows_of(gate_weight))
    hidden = (jax.nn.silu(gate_sum) * times(gathered, rows_of(up_weight))).astype(jnp.bfloat16)
    branch = times(hidden, columns_of(down_weight)).astype(jnp.bfloat16)
    summed = lax.psum_scatter(branch, "tp", scatter_dimension=0, tiled=True)
    after_first = (
        tokens.astype(jnp.float32) + 0.5 * summed.astype(jnp.float32)
    ).astype(jnp.bfloat16)
    gathered = lax.all_gather(norm_rows(after_first, mixer_gain), "tp", axis=0, tiled=True)
    queries, key_rows, value_rows = (
        times(gathered, rows_of(w)).astype(jnp.bfloat16)
        for w in (query_weight, key_weight, value_weight)
    )
    flat = retain(queries, key_rows, value_rows, head_gain, log_decay)
    branch = times(flat, columns_of(out_weight)).astype(jnp.bfloat16)
    summed = lax.psum_scatter(branch, "tp", scatter_dimension=0, tiled=True)
    return (after_first.astype(jnp.float32) + summed.astype(jnp.float32)).astype(jnp.bfloat16)


def shards(sizes, *args):
    depth = args[3].shape[0] * sizes["fs"]
    if sizes["grp"] == 2 and sizes["tp"] == 4 and depth % (2 * sizes["fs"] * LANES) == 0:
        return shards_fused(sizes["fs"], *args)
    return shards_gathered(*args)


def solution(mesh):
    placed = (
        P(("grp", "fs", "tp"), None),
        P(),
        P(),
        P("fs", "tp"),
        P("fs", "tp"),
        P("tp", "fs"),
        P("fs", "tp"),
        P("fs", "tp"),
        P("fs", "tp"),
        P("tp"),
        P("tp", "fs"),
        P(None, "tp"),
    )
    return jax.shard_map(
        functools.partial(shards, dict(mesh.shape)),
        mesh=mesh, in_specs=placed, out_specs=P(("grp", "fs", "tp"), None), check_vma=False,
    )
```

profile of v0, /device:TPU:0, one launch (start us, length us, event | category | flops | bytes accessed | tf_op | source)
XLA Modules:
  0.0 313.8 jit_solution(18110366846324901929)
XLA Ops:
  0.0 311.5 %shard_map.118 = bf16[256,2048]{1,0:T(8,128)(2,1)} custom-call(bf16[256,2048]{1,0:T(8,128)(2,1)} %refs_0_.1, f32[1,2048]{1,0:T(1,128)} %bitcast.3, f32[1,2048]{1,0:T(1,128)} %bitcast.4, f32[1,1024]{1,0:T(1,128)} %bitcast.5, f32[2,2]{1,0:T(2,128)} %refs_4_.1, bf16[512,1152]{1,0:T(8,128)(2,1)} %refs_5_.1, bf16[512,1152]{1,0:T(8,128)(2,1)} %refs_6_.1, ...), custom_call_target="tpu_custom_call" | custom-call | tf_op jit(solution)/shard_map/pallas_call | solution.py:463
  311.5 2.3 copy.14
where the time goes:
time: 314 us
  Pallas kernels  312 us (99%)
    pallas_call x1, Pallas kernels, shards_fused(): pl.pallas_call(functools.partial(layer_kernel, size), in_specs=[in_vmem]...  312 us

commit v1 on v0

--- a/solution.py
+++ b/solution.py
@@ -181,6 +181,13 @@
             def _():
                 across(w, z + k, 1 - group).wait_recv()
 
+    def arrival(place):
+        order = [sorted(range(size), key=lambda s: (abs(s - here), s)) for here in range(size)]
+        return sum(jnp.where(z == here, order[here][place], 0) for here in range(size))
+
+    def finish_shard(w, shard):
+        across(w, shard, 1 - group).wait_recv()
+
     def drain(w):
         @pl.when(z < last)
         def _():
@@ -255,45 +262,79 @@
 
         lax.fori_loop(0, weight.shape[1] // wide, tile, 0)
 
-    def scatter_far(far, base):
-        send_tp(band_of(part, (1 - chip) * 2 + (1 - core)), far, base, mate).start()
-
-    def scatter_near(near, base):
-        send_tp(band_of(part, mate), near, base + 1, mate).start()
-
-    def scatter_cross(far, pair, cross, base):
-        send_tp(far, far, base, mate).wait_recv()
+    stripe = tokens.shape[1] // size
+
+    def columns_of(shard):
+        return pl.ds(pl.multiple_of(shard * stripe, stripe), stripe)
+
+    def band_part(ref, place, shard):
+        return ref.at[pl.ds(pl.multiple_of(place * band, band), band), columns_of(shard)]
+
+    def stripe_of(ref, shard):
+        return ref.at[:, columns_of(shard)]
+
+    def scatter_stripe(source, weight, buffers, base, place):
+        far, near = buffers[:2]
+        shard = arrival(place)
+        columns = columns_of(shard)
+        for first in (far_rows, chip_rows):
+            there = pl.ds(first, half_rows)
+            part[there, columns] = dot(source[there, :], weight[:, columns]).astype(jnp.bfloat16)
+        beyond = (1 - chip) * 2 + (1 - core)
+        send_tp(
+            band_part(part, beyond, shard), stripe_of(far, shard), base + place, mate
+        ).start()
+        send_tp(
+            band_part(part, mate, shard), stripe_of(near, shard), base + size + place, mate
+        ).start()
+
+    def scatter_cross(buffers, base, place):
+        far, near, cross, pair = buffers
+        shard = arrival(place)
+        columns = columns_of(shard)
+        block = stripe_of(far, shard)
+        send_tp(block, block, base + place, mate).wait_recv()
 
         def body(first, tall):
             from_row = pl.multiple_of(peer * band + first, tall)
-            pair[pl.ds(first, tall), :] = (
-                part[pl.ds(from_row, tall), :].astype(jnp.float32)
-                + far[pl.ds(first, tall), :].astype(jnp.float32)
+            pair[pl.ds(first, tall), columns] = (
+                part[pl.ds(from_row, tall), columns].astype(jnp.float32)
+                + far[pl.ds(first, tall), columns].astype(jnp.float32)
             ).astype(jnp.bfloat16)
 
         by_chunks(body)
-        send_tp(pair, cross, base + 2, peer).start()
-
-    def scatter_end(residual, near, cross, scale, target, base):
-        send_tp(near, near, base + 1, mate).wait_recv()
-        send_tp(cross, cross, base + 2, peer).wait_recv()
-
-        def body(first, tall):
-            here = pl.ds(first, tall)
-            own_row = pl.multiple_of(spot * band + first, tall)
-            total = part[pl.ds(own_row, tall), :].astype(jnp.float32)
-            total = total + near[here, :].astype(jnp.float32)
-            total = total + cross[here, :].astype(jnp.float32)
-            target[here, :] = (
-                residual[here, :].astype(jnp.float32) + scale * total
-            ).astype(jnp.bfloat16)
-
-        by_chunks(body)
-
-    def scatter_drain(near, base):
-        for number, to in ((0, mate), (1, mate), (2, peer)):
-            send_tp(near, near, base + number, to).wait_send()
-
+        send_tp(
+            stripe_of(pair, shard), stripe_of(cross, shard), base + 2 * size + place, peer
+        ).start()
+
+    def scatter_end(residual, buffers, scale, target, base):
+        far, near, cross, pair = buffers
+        for place in range(size):
+            shard = arrival(place)
+            columns = columns_of(shard)
+            block, peer_block = stripe_of(near, shard), stripe_of(cross, shard)
+            send_tp(block, block, base + size + place, mate).wait_recv()
+            send_tp(peer_block, peer_block, base + 2 * size + place, peer).wait_recv()
+
+            def body(first, tall):
+                here = pl.ds(first, tall)
+                own_row = pl.multiple_of(spot * band + first, tall)
+                total = part[pl.ds(own_row, tall), columns].astype(jnp.float32)
+                total = total + near[here, columns].astype(jnp.float32)
+                total = total + cross[here, columns].astype(jnp.float32)
+                target[here, columns] = (
+                    residual[here, columns].astype(jnp.float32) + scale * total
+                ).astype(jnp.bfloat16)
+
+            by_chunks(body)
+
+    def scatter_drain(buffers, base):
+        for number in range(3 * size):
+            block = stripe_of(buffers[1], 0)
+            to = peer if number >= 2 * size else mate
+            send_tp(block, block, base + number, to).wait_send()
+
+    one, two = (far_one, near_one, cross_one, pair_one), (far_two, near_two, cross_two, pair_two)
     half_rows = 2 * band
     far_rows = pl.multiple_of((1 - chip) * half_rows, half_rows)
     chip_rows = pl.multiple_of(chip * half_rows, half_rows)
@@ -364,80 +405,77 @@
 
     pl.semaphore_wait(barrier, 3 + jnp.minimum(z, 1) + jnp.minimum(last - z, 1))
 
+    def pump(t):
+        for k in range(1, size):
+            w = t - k + 1
+            if 0 <= w < 7:
+                step(w, k)
+            if k == 1 and t + 2 < 7:
+                start(t + 2)
+
     start(0)
     start(1)
     normed_into(rows_one, tokens, first_gain)
     gather_start(rows_one, 0)
-    step(0, 1)
-    start(2)
-    for k in range(2, size):
-        step(0, k)
+    pump(0)
+    pump(1)
     gather_forward(rows_one, 0)
-    step(1, 1)
-    start(3)
-    for k in range(2, size):
-        step(1, k)
+    for t in range(2, size):
+        pump(t)
     gather_end(rows_one, 0)
     finish(0)
-    step(2, 1)
-    start(4)
+    pump(size)
     finish(1)
     gated_rows(0)
-    step(2, 2)
+    step(5, 1)
     gated_rows(half_rows)
+    scatter_stripe(hidden, down, one, 6, 0)
+    for k in range(2, size):
+        step(6 - k, k)
+    finish_shard(2, arrival(1))
+    scatter_stripe(hidden, down, one, 6, 1)
+    scatter_cross(one, 6, 0)
+    for place in range(2, size):
+        finish_shard(2, arrival(place))
+        scatter_stripe(hidden, down, one, 6, place)
+        scatter_cross(one, 6, place - 1)
+    scatter_cross(one, 6, size - 1)
+    step(6, 1)
+    step(5, 2)
+    scatter_end(tokens, one, 0.5, after_first, 6)
+    normed_into(rows_two, after_first, mixer_gain)
+    gather_start(rows_two, 3)
     for k in range(3, size):
-        step(2, k)
-    step(3, 1)
-    start(5)
-    finish(2)
-    product(part, hidden, down, far_rows, half_rows, 512)
-    scatter_far(far_one, 3)
-    product(part, hidden, down, chip_rows, half_rows, 512)
-    scatter_near(near_one, 3)
-    scatter_cross(far_one, pair_one, cross_one, 3)
-    for k in range(2, size):
-        step(3, k)
-    scatter_end(tokens, near_one, cross_one, 0.5, after_first, 3)
-    normed_into(rows_two, after_first, mixer_gain)
-    gather_start(rows_two, 6)
-    step(4, 1)
-    start(6)
-    for k in range(2, size):
-        step(4, k)
-    step(5, 1)
-    gather_forward(rows_two, 6)
-    step(5, 2)
-    gather_end(rows_two, 6)
+        step(7 - k, k)
+    pump(7)
+    gather_forward(rows_two, 3)
+    for t in range(8, 5 + size):
+        pump(t)
+    gather_end(rows_two, 3)
     finish(3)
     for first in (0, half_rows):
         product(queries, rows_two, query_w, first, half_rows, 512)
-    for k in range(3, size):
-        step(5, k)
-    step(6, 1)
     finish(4)
     for first in (0, half_rows):
         product(key_rows, rows_two, key_w, first, half_rows, 512)
     finish(5)
-    product(value_rows, rows_two, value_w, 0, half_rows, 512)
-    step(6, 2)
-    product(value_rows, rows_two, value_w, half_rows, half_rows, 512)
-    for k in range(3, size):
-        step(6, k)
+    for first in (0, half_rows):
+        product(value_rows, rows_two, value_w, first, half_rows, 512)
     for head in range(value_rows.shape[1] // DV):
         retain_head(head)
-    finish(6)
-    scatter_drain(near_one, 3)
-    product(part, flat, out_w, far_rows, half_rows, 512)
-    scatter_far(far_two, 9)
-    product(part, flat, out_w, chip_rows, half_rows, 512)
-    scatter_near(near_two, 9)
-    scatter_cross(far_two, pair_two, cross_two, 9)
-    scatter_end(after_first, near_two, cross_two, 1.0, updated, 9)
+    scatter_drain(one, 6)
+    scatter_stripe(flat, out_w, two, 6 + 3 * size, 0)
+    for place in range(1, size):
+        finish_shard(6, arrival(place))
+        scatter_stripe(flat, out_w, two, 6 + 3 * size, place)
+        scatter_cross(two, 6 + 3 * size, place - 1)
+    scatter_cross(two, 6 + 3 * size, size - 1)
+    scatter_end(after_first, two, 1.0, updated, 6 + 3 * size)
     for w in range(7):
         drain(w)
     gather_drain(rows_one, 0)
-    gather_drain(rows_two, 6)
-    scatter_drain(near_two, 9)
+    gather_drain(rows_two, 3)
+    scatter_drain(two, 6 + 3 * size)
 
 
 def shards_fused(
@@ -477,7 +515,7 @@
         + [held(band, depth)] * 8
         + [
             dma((count,)), dma((count, size)), dma((count, size)), dma((count,)),
-            dma((count, size)), dma((count, size)), dma((12,)), dma((12,)),
+            dma((count, size)), dma((count, size)), dma((6 + 6 * size,)), dma((6 + 6 * size,)),
         ],
         compiler_params=pltpu.CompilerParams(
             collective_id=0, has_side_effects=True, vmem_limit_bytes=67_000_000
@@ -523,7 +561,7 @@
 
 def shards(sizes, *args):
     depth = args[3].shape[0] * sizes["fs"]
-    if sizes["grp"] == 2 and sizes["tp"] == 4 and depth % (2 * sizes["fs"] * LANES) == 0:
+    if sizes["grp"] == 2 and sizes["tp"] == 4 and sizes["fs"] == 4 and depth % (2 * sizes["fs"] * LANES) == 0:
         return shards_fused(sizes["fs"], *args)
     return shards_gathered(*args)
 

time: 314 us -> 284 us (0.904)
  Pallas kernels: 312 us -> 282 us
    pallas_call x1, Pallas kernels: 312 us -> 282 us  [shards_fused(): pl.pallas_call(functools.partial(layer_kernel, size), in_specs=[in_vmem]...]
where the time goes in v1:
time: 284 us
  Pallas kernels  282 us (99%)
    pallas_call x1, Pallas kernels, shards_fused(): pl.pallas_call(functools.partial(layer_kernel, size), in_specs=[in_vmem]...  282 us

profile of v1, /device:TPU:0, one launch (start us, length us, event | category | flops | bytes accessed | tf_op | source)
XLA Modules:
  0.0 284.3 jit_solution(17098694868239996854)
XLA Ops:
  0.0 282.0 %shard_map.118 = bf16[256,2048]{1,0:T(8,128)(2,1)} custom-call(bf16[256,2048]{1,0:T(8,128)(2,1)} %refs_0_.1, f32[1,2048]{1,0:T(1,128)} %bitcast.3, f32[1,2048]{1,0:T(1,128)} %bitcast.4, f32[1,1024]{1,0:T(1,128)} %bitcast.5, f32[2,2]{1,0:T(2,128)} %refs_4_.1, bf16[512,1152]{1,0:T(8,128)(2,1)} %refs_5_.1, bf16[512,1152]{1,0:T(8,128)(2,1)} %refs_6_.1, ...), custom_call_target="tpu_custom_call" | custom-call | tf_op jit(solution)/shard_map/pallas_call | solution.py:501
  282.0 2.3 copy.14
